TPU v7x, 32 devices: a whole 2x2x4 slice. The times are simulated.
32 devices in a mesh: gr: 4 (over z), sp: 4 (over y, x), tp: 2 (over core).
Axes of the slice: x: 2, y: 2, z: 4, core: 2. Of those that a mesh axis runs over, the one named last changes fastest.
Arguments:
- prompt: bfloat16 [16, 512, 4096], P('gr', 'sp'), may hold values from -16 to 16
- forget_weight: bfloat16 [4096, 2048], P(None, 'tp'), may hold values from -0.09375 to 0.09375
- value_weight: bfloat16 [4096, 2048], P(None, 'tp'), may hold values from -0.09375 to 0.09375
- leak: float32 [2048], P('tp'), may hold values from 0 to 1, as said below
- query: bfloat16 [16, 2048], P('gr', 'tp'), may hold values from -6 to 6
- next_input: bfloat16 [16, 4096], P('gr'), may hold values from -6 to 6
- read_gain: float32 [2048], P('tp'), may hold values from 0.1 to 1.9
Outputs:
- state_cache: bfloat16 [16, 16, 128, 128], P('gr', 'tp', 'sp')
- read_out: bfloat16 [16, 2048], P('gr', 'tp')
Inputs may be any that keep to these rules, and one draw needn't show every extreme that they name: `leak`: positive, at most one half.
All inputs are finite; a program needn't handle non-finite values.
Results may differ from a plain program's by a relative error of at most 0.0062.
Values sent between devices are 32-bit elements; how exact they have to be, the bound alone decides.
A program may use at most 64 MiB of HBM per device.

v0:
```python
import jax
import jax.numpy as jnp
from jax import lax
from jax.sharding import PartitionSpec as P

DK = 128
DV = 128


def prefix(part, axis, combine, identity):
    count = lax.axis_size(axis)
    place = lax.axis_index(axis)
    ahead = count - 1 - place
    gathered = lax.all_gather(part, axis)
    state = jnp.zeros_like(part) + jnp.asarray(identity, part.dtype)

    def one(step, state):
        source = count - 1 - step
        return combine(state, lax.dynamic_index_in_dim(gathered, source, 0, False))

    return lax.fori_loop(0, ahead, one, state)


def add_decay(earlier, later_part):
    return earlier + later_part


def local(prompt, forget_weight, value_weight, leak, query, next_input, read_gain):
    seqs, span, width = prompt.shape
    heads_here = forget_weight.shape[1] // DK
    flat_rows = prompt.reshape(seqs * span, width)
    gate_pre = jnp.dot(flat_rows, forget_weight, preferred_element_type=jnp.float32).reshape(
        seqs, span, heads_here, DK
    )
    values = jnp.dot(flat_rows, value_weight, preferred_element_type=jnp.float32).astype(
        jnp.bfloat16
    )
    values = values.reshape(seqs, span, heads_here, DV)
    leak_heads = leak.reshape(heads_here, DK)
    inflow = leak_heads * jax.nn.sigmoid(-gate_pre)
    seg_cum = jnp.cumsum(jnp.log1p(-inflow), axis=1)
    seg_total = seg_cum[:, -1]
    weighted = (inflow * jnp.exp(seg_total[:, None] - seg_cum)).astype(jnp.bfloat16)
    seg_state = jnp.einsum("sphk,sphv->shkv", weighted, values, preferred_element_type=jnp.float32)
    next_pre = jnp.dot(next_input, forget_weight, preferred_element_type=jnp.float32).reshape(
        seqs, heads_here, DK
    )
    next_values = jnp.dot(next_input, value_weight, preferred_element_type=jnp.float32).astype(
        jnp.bfloat16
    )
    next_values = next_values.astype(jnp.float32).reshape(seqs, heads_here, DV)
    next_inflow = leak_heads * jax.nn.sigmoid(-next_pre)
    next_forget = 1.0 - next_inflow
    queries = query.astype(jnp.float32).reshape(seqs, heads_here, DK)
    rows_here = DK // lax.axis_size("sp")
    start = lax.axis_index("sp") * rows_here
    later = prefix(seg_total, "sp", add_decay, jnp.zeros_like(seg_total))
    term = jnp.exp(later)[..., None] * seg_state
    owned = lax.psum_scatter(term, "sp", scatter_dimension=2, tiled=True)
    forget_rows = lax.dynamic_slice_in_dim(next_forget, start, rows_here, 2)
    inflow_rows = lax.dynamic_slice_in_dim(next_inflow, start, rows_here, 2)
    query_rows = lax.dynamic_slice_in_dim(queries, start, rows_here, 2)
    read_rows = forget_rows[..., None] * owned + inflow_rows[..., None] * next_values[:, :, None, :]
    partial_read = jnp.sum(query_rows[..., None] * read_rows, axis=2)
    raw_read = lax.psum(partial_read, "sp")
    cache = owned.astype(jnp.bfloat16)
    scaled = raw_read * lax.rsqrt(jnp.mean(raw_read * raw_read, axis=-1, keepdims=True) + 1e-06)
    read_out = (
        (scaled * read_gain.reshape(heads_here, DV))
        .astype(jnp.bfloat16)
        .reshape(seqs, heads_here * DV)
    )
    return (cache, read_out)


def solution(mesh):
    placed = (
        P("gr", "sp", None),
        P(None, "tp"),
        P(None, "tp"),
        P("tp"),
        P("gr", "tp"),
        P("gr", None),
        P("tp"),
    )
    return jax.shard_map(
        local,
        mesh=mesh,
        in_specs=placed,
        out_specs=(P("gr", "tp", "sp", None), P("gr", "tp")),
        check_vma=False,
    )
```

profile of v0, /device:TPU:0, one launch (start us, length us, event | category | flops | bytes accessed | tf_op | source)
XLA Modules:
  0.0 113.5 jit_solution(14349694660606799699)
XLA Ops:
  7.2 0.0 copy-start
  7.2 0.0 reduce-scatter.2.cloned.1.call-start
  7.2 0.0 copy-start.3
  7.2 11.3 %copy.21 = bf16[1024,4096]{1,0:T(8,128)(2,1)} copy(bf16[1024,4096]{0,1:T(8,128)(2,1)} %bitcast.53) | data formatting | bytes 16777216 | tf_op jit(solution)/shard_map/dot_general | solution.py:32
  18.5 0.0 copy-done.3
  18.5 10.0 %negate_log-plus-one_fusion = (f32[4,128,8,128]{3,1,2,0:T(8,128)S(1)}, f32[4,128,8,128]{3,1,2,0:T(8,128)}) fusion(bf16[8,128,4096,1]{2,1,0,3:T(8,128)(2,1)} %bitcast.54, bf16[4,128,4096]{2,1,0:T(8,128)(2,1)} %param.9, f32[8,128]{1,0:T(8,128)S(1)} %bitcast.60), kind=kOutput, calls=%fused_computation.9 | convolution fusion | flops 4297064448 | bytes 16781312 | tf_op jit(solution)/shard_map/dot_general | solution.py:32
  28.6 1.3 %fusion.5 = f32[4,128,8,128]{3,2,1,0:T(8,128)S(1)} fusion(f32[4,128,8,128]{3,1,2,0:T(8,128)S(1)} %get-tuple-element.73), kind=kOutput, calls=%fused_computation.7 | output fusion | flops 66584576 | bytes 4194304 | tf_op jit(solution)/shard_map/jit(cumsum)/reduce_window_sum | solution.py:41
  29.9 9.7 %all-gather = f32[16,1,8,128]{3,2,1,0:T(8,128)S(1)} all-gather(f32[4,1,8,128]{3,2,1,0:T(8,128)S(1)} %get-tuple-element.69), channel_id=2, replica_groups=mesh['gr'=4,'sp'=4,'tp'=2] {'sp'}, dimensions={0}, use_global_device_ids=true | all-gather | bytes 81920 | tf_op jit(solution)/shard_map/all_gather | solution.py:14
  39.6 0.1 while.12
  39.7 9.1 %fusion.9 = bf16[64,8,8,128]{3,1,2,0:T(8,128)(2,1)S(1)} fusion(bf16[512,4096]{1,0:T(8,128)(2,1)} %bitcast.63, bf16[4096,1024]{1,0:T(8,128)(2,1)} %param.11), kind=kOutput, calls=%fused_computation.13 | convolution fusion | flops 4295491584 | bytes 13631488 | tf_op jit(solution)/shard_map/dot_general | solution.py:35
  48.9 0.0 copy-start.1
  48.9 0.3 copy.22
  49.2 1.3 %copy-done.1 = f32[4,128,8,128]{3,1,2,0:T(8,128)S(1)} copy-done((f32[4,128,8,128]{3,1,2,0:T(8,128)S(1)}, f32[4,128,8,128]{3,1,2,0:T(8,128)}, u32[]{:S(2)}) %copy-start.1) | copy-done | bytes 2097176
  50.5 2.3 %convolution_multiply_fusion = f32[4,8,128,128]{3,2,1,0:T(8,128)} fusion(f32[4,128,8,128]{3,1,2,0:T(8,128)S(1)} %copy-done.1, f32[4,128,8,128]{3,2,1,0:T(8,128)S(1)} %fusion.5, bf16[4,128,8,128]{3,2,1,0:T(8,128)(2,1)S(1)} %bitcast.55, f32[4,8,128]{2,1,0:T(8,128)S(1)} %get-tuple-element.70, f32[4,8,128]{2,1,0:T(8,128)S(1)} %exp.14), kind=kOutput, calls=%fused_computation.11 | convolution fusion | flops 136314880 | bytes 7372800 | tf_op jit(solution)/shard_map/sphk,sphv->shkv/dot_general | solution.py:44
  52.7 0.0 copy-start.2
  52.7 0.0 reduce-scatter.2.cloned.1.call-update
  52.8 0.7 copy-done.2
  53.5 0.0 copy-done
  53.5 4.6 %fusion.14 = f32[1,4,8,128]{3,1,2,0:T(4,128)S(1)} fusion(bf16[4,4096]{1,0:T(4,128)(2,1)S(1)} %copy-done, bf16[4096,1024]{1,0:T(8,128)(2,1)} %param.11), kind=kOutput, calls=%fused_computation.20 | convolution fusion | flops 33562624 | bytes 8437760 | tf_op jit(solution)/shard_map/dot_general | solution.py:48
  58.0 0.0 copy-start.4
  58.0 5.0 %fusion.12 = f32[1,4,8,128]{3,1,2,0:T(4,128)S(1)} fusion(bf16[4,4096]{1,0:T(4,128)(2,1)S(1)} %copy-done, bf16[4096,1024]{1,0:T(8,128)(2,1)} %param.10), kind=kOutput, calls=%fused_computation.17 | convolution fusion | flops 33562624 | bytes 8437760 | tf_op jit(solution)/shard_map/dot_general | solution.py:45
  63.0 0.1 broadcast_subtract_fusion
  63.1 25.3 %reduce-scatter.2.cloned.1.call-done = f32[4,8,32,128]{3,2,1,0:T(8,128)} async-done(((f32[4,8,128,128]{3,2,1,0:T(8,128)}), f32[4,8,32,128]{3,2,1,0:T(8,128)}) %reduce-scatter.2.cloned.1.call-update) | async-done | bytes 524304 | tf_op jit(solution)/shard_map/reduce_scatter | solution.py:59
  88.4 2.4 %multiply_reduce_fusion = (f32[4,8,128]{2,1,0:T(8,128)S(1)}, bf16[4,8,32,128]{3,2,1,0:T(8,128)(2,1)}) fusion(f32[4,8,32,128]{3,2,1,0:T(8,128)} %reduce-scatter.2.cloned.1.call-done, f32[4,8,128]{2,1,0:T(8,128)S(1)} %bitcast.57, f32[4,8,32]{2,1,0:T(8,128)S(1)} %get-tuple-element.68, f32[4,8,32]{2,1,0:T(8,128)S(1)} %get-tuple-element.67, ...), kind=kLoop, calls=%fused_computation.23 | loop fusion | flops 782336 | bytes 831488 | tf_op jit(solution)/shard_map/reduce_sum | solution.py:64
  90.7 15.1 %psum.7 = f32[4,8,128]{2,1,0:T(8,128)S(1)} all-reduce(f32[4,8,128]{2,1,0:T(8,128)S(1)} %get-tuple-element.71), channel_id=1, replica_groups=mesh['gr'=4,'sp'=4,'tp'=2] {'sp'}, use_global_device_ids=true, to_apply=%region_5.6 | all-reduce | flops 4096 | bytes 32768 | tf_op jit(solution)/shard_map/psum | solution.py:65
  105.8 0.1 multiply_reduce_fusion.1
  105.9 0.0 copy-done.4
  105.9 0.1 fusion.18
  106.0 0.6 copy.45
  (11 shorter events, 0.1 us)
Async XLA Ops:
  7.2 46.3 %copy-start = (bf16[4,4096]{1,0:T(4,128)(2,1)S(1)}, bf16[4,4096]{1,0:T(4,128)(2,1)}, u32[]{:S(2)}) copy-start(bf16[4,4096]{1,0:T(4,128)(2,1)} %param.14) | copy-start | bytes 98308
  7.2 81.2 %reduce-scatter.2.cloned.1.call-start = ((), (), s32[]{:S(2)}) async-start(), calls=%async_computation.1 | async-start | bytes 2621440 | tf_op jit(solution)/shard_map/reduce_scatter | solution.py:59
  7.2 11.3 %copy-start.3 = (f32[1024]{0:T(1024)S(1)}, f32[1024]{0:T(1024)}, u32[]{:S(2)}) copy-start(f32[1024]{0:T(1024)} %param.12) | copy-start | bytes 12292
  48.9 1.6 %copy-start.1 = (f32[4,128,8,128]{3,1,2,0:T(8,128)S(1)}, f32[4,128,8,128]{3,1,2,0:T(8,128)}, u32[]{:S(2)}) copy-start(f32[4,128,8,128]{3,1,2,0:T(8,128)} %get-tuple-element.74) | copy-start | bytes 6291460
  52.7 0.7 copy-start.2
  58.0 47.9 %copy-start.4 = (f32[1024]{0:T(1024)S(1)}, f32[1024]{0:T(1024)}, u32[]{:S(2)}) copy-start(f32[1024]{0:T(1024)} %param.15) | copy-start | bytes 12292
Sparse Core Ops, SparseCore 0:
  52.9 35.4 reduce-scatter.1
where the time goes:
time: 114 us; the launch traced here: 113 us
  matrix products  31 us (27%)
  waiting for transfers between devices  25.3 us (22%)
  blocking collectives  24.8 us (22%)
  local copies, waits for them, and re-layouts  14.2 us (12%)
  between operations  14.1 us (12%)
  other arithmetic  3.95 us (3%)
    reduce_scatter x1, waiting for transfers between devices, local(): owned = lax.psum_scatter(term, 'sp', scatter_dimension=2, tiled=True)  25.3 us
    psum x1, blocking collectives, local(): raw_read = lax.psum(partial_read, 'sp')  15.1 us
    dot_general x1, local copies, waits for them, and re-layouts, local(): jnp.dot(flat_rows, forget_weight, preferred_element_type=jnp.float32)  11.3 us
    dot_general x1, matrix products, local(): jnp.dot(flat_rows, forget_weight, preferred_element_type=jnp.float32)  10 us
    all_gather x1, blocking collectives, prefix(): gathered = lax.all_gather(part, axis)  9.72 us
    dot_general x1, matrix products, local(): jnp.dot(flat_rows, value_weight, preferred_element_type=jnp.float32)  9.15 us
    dot_general x1, matrix products, local(): jnp.dot(next_input, forget_weight, preferred_element_type=jnp.float32)  4.95 us
    dot_general x1, matrix products, local(): jnp.dot(next_input, value_weight, preferred_element_type=jnp.float32)  4.57 us
  transfers between devices with their start and end apart: 1, of which 1 were waited for; matrix products, arithmetic and copies ran while one was open for 8% of the time, Pallas kernels for 0%

commit v1 on v0

--- a/solution.py
+++ b/solution.py
@@ -1,10 +1,262 @@
+import functools
+
 import jax
 import jax.numpy as jnp
 from jax import lax
+from jax.experimental import pallas as pl
+from jax.experimental.pallas import tpu as pltpu
 from jax.sharding import PartitionSpec as P
 
 DK = 128
 DV = 128
+PAIR = 2
+PAD = 16
+F32 = jnp.float32
+BF16 = jnp.bfloat16
+
+
+def suffix_product(x):
+    rows = x.shape[0]
+    step = 1
+    while step < rows:
+        x = x * jnp.concatenate([x[step:], jnp.ones((step, x.shape[1]), F32)], axis=0)
+        step *= 2
+    return x
+
+
+def kernel(
+    seqs, span, chunks,
+    prompt, forget_w, value_w, leak, query, nxt, gain,
+    cache, read_out,
+    x_v, fw_v, vw_v, pad_v, gate_v, val_v, keys_v, qf_v, qi_v, nv_v,
+    totals, states, stage1, stage2, reads,
+    load_sem, tot_s, tot_r, s1_s, s1_r, s2_s, s2_r, rd_s, rd_r,
+):
+    me = lax.axis_index("sp")
+    count = 4
+    xbit, ybit = me % 2, me // 2
+    xpeer = me + 1 - 2 * xbit
+    ypeer = me + 2 - 4 * ybit
+    dpeer = 3 - me
+    peers = (xpeer, ypeer, dpeer)
+    rows = seqs * span
+    wide = PAIR * DK
+    kdev = DK // count
+
+    def cols(c):
+        return slice(c * wide, (c + 1) * wide)
+
+    def load_w(c, which):
+        src, dst = ((forget_w, fw_v), (value_w, vw_v))[which]
+        return pltpu.make_async_copy(
+            src.at[:, cols(c)], dst.at[:, cols(c)], load_sem.at[1 + 2 * c + which]
+        )
+
+    load_x = pltpu.make_async_copy(prompt, x_v.at[pl.ds(0, rows)], load_sem.at[0])
+    load_x.start()
+    load_w(0, 0).start()
+    for c in range(chunks):
+        if c + 1 < chunks:
+            load_w(c + 1, 0).start()
+        load_w(c, 1).start()
+
+    barrier = pltpu.get_barrier_semaphore()
+    for peer in peers:
+        pl.semaphore_signal(barrier, inc=1, device_id={"sp": peer})
+    pad_v[...] = jnp.zeros_like(pad_v)
+    pad_v[0:seqs, :] = nxt[...].astype(F32)
+    x_v[rows:, :] = pad_v[...].astype(BF16)
+    pl.semaphore_wait(barrier, 3)
+
+    def tot_copy(c, i):
+        return pltpu.make_async_remote_copy(
+            src_ref=totals.at[c, me], dst_ref=totals.at[c, me],
+            send_sem=tot_s.at[c, i], recv_sem=tot_r.at[c, i],
+            device_id={"sp": peers[i]},
+        )
+
+    def read_copy(i):
+        return pltpu.make_async_remote_copy(
+            src_ref=reads.at[me], dst_ref=reads.at[me],
+            send_sem=rd_s.at[i], recv_sem=rd_r.at[i],
+            device_id={"sp": peers[i]},
+        )
+
+    def s1_copy(c, j):
+        bit, peer = ((xbit, xpeer), (ybit, ypeer))[j]
+        return pltpu.make_async_remote_copy(
+            src_ref=states.at[c, j, 1 - bit], dst_ref=stage1.at[c, j],
+            send_sem=s1_s.at[c, j], recv_sem=s1_r.at[c, j],
+            device_id={"sp": peer},
+        )
+
+    def s2_copy(c, j):
+        bit, (bit2, peer) = ((xbit, (ybit, ypeer)), (ybit, (xbit, xpeer)))[j]
+        return pltpu.make_async_remote_copy(
+            src_ref=states.at[c, j, bit, 1 - bit2], dst_ref=stage2.at[c, j],
+            send_sem=s2_s.at[c, j], recv_sem=s2_r.at[c, j],
+            device_id={"sp": peer},
+        )
+
+    def gates(c):
+        load_w(c, 0).wait()
+        gate_v[...] = jnp.dot(x_v[...], fw_v[:, cols(c)], preferred_element_type=F32)
+        lk = leak[:, cols(c)]
+        for s in range(seqs):
+            at = slice(s * span, (s + 1) * span)
+            inflow = lk * jax.nn.sigmoid(-gate_v[at, :])
+            forget = 1.0 - inflow
+            after = suffix_product(
+                jnp.concatenate([forget[1:], jnp.ones((1, wide), F32)], axis=0)
+            )
+            keys_v[c % 2, at, :] = inflow * after
+            totals[c, me, s : s + 1, :] = forget[0:1] * after[0:1]
+        n_in = lk * jax.nn.sigmoid(-gate_v[rows : rows + seqs, :])
+        q = query[:, cols(c)].astype(F32)
+        qf_v[:, cols(c)] = q * (1.0 - n_in)
+        qi_v[:, cols(c)] = q * n_in
+        for i in range(3):
+            tot_copy(c, i).start()
+
+    def segment_states(c):
+        load_w(c, 1).wait()
+        val_v[...] = jnp.dot(x_v[...], vw_v[:, cols(c)], preferred_element_type=F32).astype(BF16)
+        nv_v[:, cols(c)] = val_v[rows:, :].astype(F32)
+        for i in range(3):
+            tot_copy(c, i).wait_recv()
+        later = jnp.ones((seqs, wide), F32)
+        for source in range(1, count):
+            part = totals[c, source, 0:seqs, :]
+            later = later * jnp.where(source > me, part, jnp.ones_like(part))
+        for s in range(seqs):
+            at = slice(s * span, (s + 1) * span)
+            weighted = (keys_v[c % 2, at, :] * later[s : s + 1]).astype(BF16)
+            weighed = weighted.astype(F32) * qf_v[s : s + 1, cols(c)]
+            for j in range(PAIR):
+                head = slice(j * DK, (j + 1) * DK)
+                v = val_v[at, head]
+                state = lax.dot_general(
+                    weighted[:, head], v, (((0,), (0,)), ((), ())),
+                    preferred_element_type=F32,
+                )
+                for owner in range(count):
+                    first, second = (owner % 2, owner // 2)[:: 1 if j == 0 else -1]
+                    states[c, j, first, second, s * kdev : (s + 1) * kdev, :] = state[
+                        owner * kdev : (owner + 1) * kdev
+                    ]
+                a = jnp.sum(weighed[:, head], axis=1, keepdims=True)
+                reads[me, s : s + 1, c * wide + j * DV : c * wide + (j + 1) * DV] = jnp.sum(
+                    a * v.astype(F32), axis=0, keepdims=True
+                )
+        for j in range(PAIR):
+            s1_copy(c, j).start()
+
+    def combine(c):
+        for j in range(PAIR):
+            bit = (xbit, ybit)[j]
+            s1_copy(c, j).wait_recv()
+            states[c, j, bit] = states[c, j, bit] + stage1[c, j]
+            s2_copy(c, j).start()
+
+    def finish(c):
+        for j in range(PAIR):
+            bit, bit2 = ((xbit, ybit), (ybit, xbit))[j]
+            s2_copy(c, j).wait_recv()
+            owned = states[c, j, bit, bit2] + stage2[c, j]
+            for s in range(seqs):
+                cache[s, c * PAIR + j] = owned[s * kdev : (s + 1) * kdev].astype(BF16)
+
+    load_x.wait()
+    gates(0)
+    for c in range(chunks):
+        if c + 1 < chunks:
+            gates(c + 1)
+        segment_states(c)
+        if c + 1 == chunks:
+            for i in range(3):
+                read_copy(i).start()
+        if c >= 1:
+            combine(c - 1)
+        if c >= 2:
+            finish(c - 2)
+    combine(chunks - 1)
+    for i in range(3):
+        read_copy(i).wait_recv()
+    raw = reads[0]
+    for source in range(1, count):
+        raw = raw + reads[source]
+    for h in range(chunks * PAIR):
+        head = slice(h * DV, (h + 1) * DV)
+        inner = jnp.sum(qi_v[:, head], axis=1, keepdims=True)
+        r = raw[0:seqs, head] + inner * nv_v[0:seqs, head]
+        scale = lax.rsqrt(jnp.mean(r * r, axis=1, keepdims=True) + 1e-06)
+        read_out[:, head] = (r * scale * gain[:, head]).astype(BF16)
+    for c in range(max(chunks - 2, 0), chunks):
+        finish(c)
+    for c in range(chunks):
+        for i in range(3):
+            tot_copy(c, i).wait_send()
+        for j in range(PAIR):
+            s1_copy(c, j).wait_send()
+            s2_copy(c, j).wait_send()
+    for i in range(3):
+        read_copy(i).wait_send()
+
+
+def fused(prompt, forget_weight, value_weight, leak, query, next_input, read_gain):
+    seqs, span, width = prompt.shape
+    here = forget_weight.shape[1]
+    heads = here // DK
+    chunks = heads // PAIR
+    wide = PAIR * DK
+    count = lax.axis_size("sp")
+    kdev = DK // count
+    rows = seqs * span
+    srows = -(-seqs // 8) * 8
+    anyspace = pl.BlockSpec(memory_space=pl.ANY)
+    vm = pl.BlockSpec(memory_space=pltpu.VMEM)
+    dma = pltpu.SemaphoreType.DMA
+    return pl.pallas_call(
+        functools.partial(kernel, seqs, span, chunks),
+        out_shape=(
+            jax.ShapeDtypeStruct((seqs, heads, kdev, DV), BF16),
+            jax.ShapeDtypeStruct((seqs, here), BF16),
+        ),
+        in_specs=[anyspace, anyspace, anyspace, vm, vm, vm, vm],
+        out_specs=(vm, vm),
+        scratch_shapes=[
+            pltpu.VMEM((rows + PAD, width), BF16),
+            pltpu.VMEM((width, here), BF16),
+            pltpu.VMEM((width, here), BF16),
+            pltpu.VMEM((PAD, width), F32),
+            pltpu.VMEM((rows + PAD, wide), F32),
+            pltpu.VMEM((rows + PAD, wide), BF16),
+            pltpu.VMEM((2, rows, wide), F32),
+            pltpu.VMEM((seqs, here), F32),
+            pltpu.VMEM((seqs, here), F32),
+            pltpu.VMEM((PAD, here), F32),
+            pltpu.VMEM((chunks, count, srows, wide), F32),
+            pltpu.VMEM((chunks, PAIR, 2, 2, seqs * kdev, DV), F32),
+            pltpu.VMEM((chunks, PAIR, 2, seqs * kdev, DV), F32),
+            pltpu.VMEM((chunks, PAIR, seqs * kdev, DV), F32),
+            pltpu.VMEM((count, srows, here), F32),
+            dma((1 + 2 * chunks,)),
+            dma((chunks, 3)),
+            dma((chunks, 3)),
+            dma((chunks, PAIR)),
+            dma((chunks, PAIR)),
+            dma((chunks, PAIR)),
+            dma((chunks, PAIR)),
+            dma((3,)),
+            dma((3,)),
+        ],
+        compiler_params=pltpu.CompilerParams(
+            collective_id=0, has_side_effects=True, vmem_limit_bytes=60 * 1024 * 1024
+        ),
+    )(
+        prompt.reshape(rows, width), forget_weight, value_weight, leak.reshape(1, here),
+        query, next_input, read_gain.reshape(1, here),
+    )
 
 
 def prefix(part, axis, combine, identity):
@@ -84,7 +336,7 @@
         P("tp"),
     )
     return jax.shard_map(
-        local,
+        fused if mesh.shape["sp"] == 4 else local,
         mesh=mesh,
         in_specs=placed,
         out_specs=(P("gr", "tp", "sp", None), P("gr", "tp")),

time: 114 us -> 43.1 us (0.38)
  Pallas kernels: 0 us -> 39.2 us
  matrix products: 31 us -> 0 us
  waiting for transfers between devices: 25.3 us -> 0 us
  blocking collectives: 24.8 us -> 0 us
  between operations: 14.1 us -> 0.64 us
  local copies, waits for them, and re-layouts: 14.2 us -> 2.97 us
  other arithmetic: 3.95 us -> 0 us
    pallas_call x0 -> x1, Pallas kernels: none -> 39.2 us  [fused(): pl.pallas_call(functools.partial(kernel, seqs, span, chunks), out_shape=(...]
    dot_general x5 -> x0, matrix products: 31 us -> none  [the longest x1 10 us: local(): jnp.dot(flat_rows, forget_weight, preferred_element_type=jnp.float32)]
    reduce_scatter x1 -> x0, waiting for transfers between devices: 25.3 us -> none  [local(): owned = lax.psum_scatter(term, 'sp', scatter_dimension=2, tiled=True)]
    psum x1 -> x0, blocking collectives: 15.1 us -> none  [local(): raw_read = lax.psum(partial_read, 'sp')]
    dot_general x1 -> x0, local copies, waits for them, and re-layouts: 11.3 us -> none  [local(): jnp.dot(flat_rows, forget_weight, preferred_element_type=jnp.float32)]
    all_gather x1 -> x0, blocking collectives: 9.72 us -> none  [prefix(): gathered = lax.all_gather(part, axis)]
    reduce_sum x2 -> x0, other arithmetic: 2.47 us -> none  [the longest x1 2.38 us: local(): partial_read = jnp.sum(query_rows[..., None] * read_rows, axis=2)]
    another operation x1 -> x0, other arithmetic: 1.28 us -> none  [local(): seg_cum = jnp.cumsum(jnp.log1p(-inflow), axis=1)]
  transfers between devices with their start and end apart: 1 -> 0, of which waited for: 1 -> 0; matrix products, arithmetic and copies ran while one was open for 8% -> 0% of each run, Pallas kernels for 0% -> 0%
where the time goes in v1:
time: 43.1 us; the launch traced here: 42.8 us
  Pallas kernels  39.2 us (91%)
  local copies, waits for them, and re-layouts  2.97 us (7%)
  between operations  0.64 us (1%)
    pallas_call x1, Pallas kernels, fused(): pl.pallas_call(functools.partial(kernel, seqs, span, chunks), out_shape=(...  39.2 us
    unnamed x2, local copies, waits for them, and re-layouts  2.97 us

profile of v1, /device:TPU:0, one launch (start us, length us, event | category | flops | bytes accessed | tf_op | source)
XLA Modules:
  0.0 42.8 jit_solution(12961086979361907158)
XLA Ops:
  0.6 39.2 %shard_map.86 = (bf16[4,8,32,128]{3,2,1,0:T(8,128)(2,1)}, bf16[4,1024]{1,0:T(4,128)(2,1)}) custom-call(bf16[512,4096]{1,0:T(8,128)(2,1)} %bitcast.3, bf16[4096,1024]{1,0:T(8,128)(2,1)} %forget_w.1, bf16[4096,1024]{1,0:T(8,128)(2,1)} %value_w.1, f32[1,1024]{1,0:T(1,128)} %bitcast.4, bf16[4,1024]{1,0:T(4,128)(2,1)} %query.1, bf16[4,4096]{1,0:T(4,128)(2,1)} %nxt.1, ...), custom_call_target="tpu_custom_call" | custom-call | tf_op jit(solution)/shard_map/pallas_call | solution.py:219
  39.8 1.7 %copy.11 = bf16[4,8,32,128]{3,2,1,0:T(8,128)(2,1)} copy(bf16[4,8,32,128]{3,2,1,0:T(8,128)(2,1)} %get-tuple-element.4) | data formatting | bytes 524288
  41.5 1.3 %copy.12 = bf16[4,1024]{1,0:T(4,128)(2,1)} copy(bf16[4,1024]{1,0:T(4,128)(2,1)} %get-tuple-element.5) | data formatting | bytes 16384

commit v2 on v1

--- a/solution.py
+++ b/solution.py
@@ -44,7 +44,7 @@
     kdev = DK // count
 
     def cols(c):
-        return slice(c * wide, (c + 1) * wide)
+        return pl.ds(pl.multiple_of(c * wide, wide), wide)
 
     def load_w(c, which):
         src, dst = ((forget_w, fw_v), (value_w, vw_v))[which]
@@ -145,7 +145,7 @@
                         owner * kdev : (owner + 1) * kdev
                     ]
                 a = jnp.sum(weighed[:, head], axis=1, keepdims=True)
-                reads[me, s : s + 1, c * wide + j * DV : c * wide + (j + 1) * DV] = jnp.sum(
+                reads[me, s : s + 1, pl.ds(pl.multiple_of(c * wide + j * DV, DV), DV)] = jnp.sum(
                     a * v.astype(F32), axis=0, keepdims=True
                 )
         for j in range(PAIR):
@@ -167,19 +167,32 @@
                 cache[s, c * PAIR + j] = owned[s * kdev : (s + 1) * kdev].astype(BF16)
 
     load_x.wait()
-    gates(0)
-    for c in range(chunks):
-        if c + 1 < chunks:
-            gates(c + 1)
-        segment_states(c)
-        if c + 1 == chunks:
-            for i in range(3):
-                read_copy(i).start()
-        if c >= 1:
-            combine(c - 1)
-        if c >= 2:
-            finish(c - 2)
-    combine(chunks - 1)
+
+    def stage(i, carry):
+        @pl.when(i < chunks)
+        def _():
+            gates(i)
+
+        @pl.when((i >= 1) & (i <= chunks))
+        def _():
+            segment_states(i - 1)
+
+        @pl.when(i == chunks)
+        def _():
+            for p in range(3):
+                read_copy(p).start()
+
+        @pl.when((i >= 2) & (i <= chunks + 1))
+        def _():
+            combine(i - 2)
+
+        @pl.when(i >= 3)
+        def _():
+            finish(i - 3)
+
+        return carry
+
+    lax.fori_loop(0, chunks + 2, stage, 0)
     for i in range(3):
         read_copy(i).wait_recv()
     raw = reads[0]
@@ -191,8 +204,7 @@
         r = raw[0:seqs, head] + inner * nv_v[0:seqs, head]
         scale = lax.rsqrt(jnp.mean(r * r, axis=1, keepdims=True) + 1e-06)
         read_out[:, head] = (r * scale * gain[:, head]).astype(BF16)
-    for c in range(max(chunks - 2, 0), chunks):
-        finish(c)
+    finish(chunks - 1)
     for c in range(chunks):
         for i in range(3):
             tot_copy(c, i).wait_send()

time: 43.1 us -> 37.3 us (0.87)
  Pallas kernels: 39.2 us -> 33.4 us
    pallas_call x1, Pallas kernels: 39.2 us -> 33.4 us  [fused(): pl.pallas_call(functools.partial(kernel, seqs, span, chunks), out_shape=(...]
where the time goes in v2:
time: 37.3 us; the launch traced here: 37.1 us
  Pallas kernels  33.4 us (90%)
  local copies, waits for them, and re-layouts  2.97 us (8%)
  between operations  0.64 us (2%)
    pallas_call x1, Pallas kernels, fused(): pl.pallas_call(functools.partial(kernel, seqs, span, chunks), out_shape=(...  33.4 us
    unnamed x2, local copies, waits for them, and re-layouts  2.97 us

profile of v2, /device:TPU:0, one launch (start us, length us, event | category | flops | bytes accessed | tf_op | source)
XLA Modules:
  0.0 37.1 jit_solution(1382003886539255872)
XLA Ops:
  0.6 33.4 %shard_map.86 = (bf16[4,8,32,128]{3,2,1,0:T(8,128)(2,1)}, bf16[4,1024]{1,0:T(4,128)(2,1)}) custom-call(bf16[512,4096]{1,0:T(8,128)(2,1)} %bitcast.3, bf16[4096,1024]{1,0:T(8,128)(2,1)} %forget_w.1, bf16[4096,1024]{1,0:T(8,128)(2,1)} %value_w.1, f32[1,1024]{1,0:T(1,128)} %bitcast.4, bf16[4,1024]{1,0:T(4,128)(2,1)} %query.1, bf16[4,4096]{1,0:T(4,128)(2,1)} %nxt.1, ...), custom_call_target="tpu_custom_call" | custom-call | tf_op jit(solution)/shard_map/pallas_call | solution.py:231
  34.1 1.7 %copy.11 = bf16[4,8,32,128]{3,2,1,0:T(8,128)(2,1)} copy(bf16[4,8,32,128]{3,2,1,0:T(8,128)(2,1)} %get-tuple-element.4) | data formatting | bytes 524288
  35.8 1.3 %copy.12 = bf16[4,1024]{1,0:T(4,128)(2,1)} copy(bf16[4,1024]{1,0:T(4,128)(2,1)} %get-tuple-element.5) | data formatting | bytes 16384

commit v3 on v2

--- a/solution.py
+++ b/solution.py
@@ -11,6 +11,7 @@
 DV = 128
 PAIR = 2
 PAD = 16
+LAG = 3
 F32 = jnp.float32
 BF16 = jnp.bfloat16
 
@@ -75,10 +76,10 @@
             device_id={"sp": peers[i]},
         )
 
-    def read_copy(i):
+    def read_copy(c, i):
         return pltpu.make_async_remote_copy(
-            src_ref=reads.at[me], dst_ref=reads.at[me],
-            send_sem=rd_s.at[i], recv_sem=rd_r.at[i],
+            src_ref=reads.at[c, me], dst_ref=reads.at[c, me],
+            send_sem=rd_s.at[c, i], recv_sem=rd_r.at[c, i],
             device_id={"sp": peers[i]},
         )
 
@@ -110,7 +111,9 @@
                 jnp.concatenate([forget[1:], jnp.ones((1, wide), F32)], axis=0)
             )
             keys_v[c % 2, at, :] = inflow * after
-            totals[c, me, s : s + 1, :] = forget[0:1] * after[0:1]
+            total = forget[0:1] * after[0:1]
+            for j in range(PAIR):
+                totals[c, me, j * seqs + s : j * seqs + s + 1, :] = total[:, j * DK : (j + 1) * DK]
         n_in = lk * jax.nn.sigmoid(-gate_v[rows : rows + seqs, :])
         q = query[:, cols(c)].astype(F32)
         qf_v[:, cols(c)] = q * (1.0 - n_in)
@@ -124,13 +127,16 @@
         nv_v[:, cols(c)] = val_v[rows:, :].astype(F32)
         for i in range(3):
             tot_copy(c, i).wait_recv()
-        later = jnp.ones((seqs, wide), F32)
+        later = jnp.ones((PAIR * seqs, DK), F32)
         for source in range(1, count):
-            part = totals[c, source, 0:seqs, :]
+            part = totals[c, source]
             later = later * jnp.where(source > me, part, jnp.ones_like(part))
         for s in range(seqs):
             at = slice(s * span, (s + 1) * span)
-            weighted = (keys_v[c % 2, at, :] * later[s : s + 1]).astype(BF16)
+            to_end = jnp.concatenate(
+                [later[j * seqs + s : j * seqs + s + 1] for j in range(PAIR)], axis=1
+            )
+            weighted = (keys_v[c % 2, at, :] * to_end).astype(BF16)
             weighed = weighted.astype(F32) * qf_v[s : s + 1, cols(c)]
             for j in range(PAIR):
                 head = slice(j * DK, (j + 1) * DK)
@@ -145,11 +151,13 @@
                         owner * kdev : (owner + 1) * kdev
                     ]
                 a = jnp.sum(weighed[:, head], axis=1, keepdims=True)
-                reads[me, s : s + 1, pl.ds(pl.multiple_of(c * wide + j * DV, DV), DV)] = jnp.sum(
+                reads[c, me, j * seqs + s : j * seqs + s + 1, :] = jnp.sum(
                     a * v.astype(F32), axis=0, keepdims=True
                 )
         for j in range(PAIR):
             s1_copy(c, j).start()
+        for i in range(3):
+            read_copy(c, i).start()
 
     def combine(c):
         for j in range(PAIR):
@@ -173,37 +181,33 @@
         def _():
             gates(i)
 
-        @pl.when((i >= 1) & (i <= chunks))
+        @pl.when(i >= 1)
         def _():
             segment_states(i - 1)
 
-        @pl.when(i == chunks)
+        @pl.when(i >= LAG)
         def _():
-            for p in range(3):
-                read_copy(p).start()
-
-        @pl.when((i >= 2) & (i <= chunks + 1))
-        def _():
-            combine(i - 2)
-
-        @pl.when(i >= 3)
-        def _():
-            finish(i - 3)
+            combine(i - LAG)
 
         return carry
 
-    lax.fori_loop(0, chunks + 2, stage, 0)
-    for i in range(3):
-        read_copy(i).wait_recv()
-    raw = reads[0]
-    for source in range(1, count):
-        raw = raw + reads[source]
-    for h in range(chunks * PAIR):
-        head = slice(h * DV, (h + 1) * DV)
-        inner = jnp.sum(qi_v[:, head], axis=1, keepdims=True)
-        r = raw[0:seqs, head] + inner * nv_v[0:seqs, head]
-        scale = lax.rsqrt(jnp.mean(r * r, axis=1, keepdims=True) + 1e-06)
-        read_out[:, head] = (r * scale * gain[:, head]).astype(BF16)
+    lax.fori_loop(0, chunks + 1, stage, 0)
+    for c in range(chunks + 1 - LAG, chunks):
+        combine(c)
+    for c in range(chunks - 1):
+        finish(c)
+    for c in range(chunks):
+        for i in range(3):
+            read_copy(c, i).wait_recv()
+        raw = reads[c, 0]
+        for source in range(1, count):
+            raw = raw + reads[c, source]
+        for j in range(PAIR):
+            head = slice((c * PAIR + j) * DV, (c * PAIR + j + 1) * DV)
+            inner = jnp.sum(qi_v[:, head], axis=1, keepdims=True)
+            r = raw[j * seqs : (j + 1) * seqs] + inner * nv_v[0:seqs, head]
+            scale = lax.rsqrt(jnp.mean(r * r, axis=1, keepdims=True) + 1e-06)
+            read_out[:, head] = (r * scale * gain[:, head]).astype(BF16)
     finish(chunks - 1)
     for c in range(chunks):
         for i in range(3):
@@ -211,8 +215,13 @@
         for j in range(PAIR):
             s1_copy(c, j).wait_send()
             s2_copy(c, j).wait_send()
-    for i in range(3):
-        read_copy(i).wait_send()
+        for i in range(3):
+            read_copy(c, i).wait_send()
+
+
+def hand_over(cache_in, read_in, cache, read_out):
+    cache[...] = cache_in[...]
+    read_out[...] = read_in[...]
 
 
 def fused(prompt, forget_weight, value_weight, leak, query, next_input, read_gain):
@@ -224,11 +233,10 @@
     count = lax.axis_size("sp")
     kdev = DK // count
     rows = seqs * span
-    srows = -(-seqs // 8) * 8
     anyspace = pl.BlockSpec(memory_space=pl.ANY)
     vm = pl.BlockSpec(memory_space=pltpu.VMEM)
     dma = pltpu.SemaphoreType.DMA
-    return pl.pallas_call(
+    made = pl.pallas_call(
         functools.partial(kernel, seqs, span, chunks),
         out_shape=(
             jax.ShapeDtypeStruct((seqs, heads, kdev, DV), BF16),
@@ -247,11 +255,11 @@
             pltpu.VMEM((seqs, here), F32),
             pltpu.VMEM((seqs, here), F32),
             pltpu.VMEM((PAD, here), F32),
-            pltpu.VMEM((chunks, count, srows, wide), F32),
+            pltpu.VMEM((chunks, count, PAIR * seqs, DK), F32),
             pltpu.VMEM((chunks, PAIR, 2, 2, seqs * kdev, DV), F32),
             pltpu.VMEM((chunks, PAIR, 2, seqs * kdev, DV), F32),
             pltpu.VMEM((chunks, PAIR, seqs * kdev, DV), F32),
-            pltpu.VMEM((count, srows, here), F32),
+            pltpu.VMEM((chunks, count, PAIR * seqs, DV), F32),
             dma((1 + 2 * chunks,)),
             dma((chunks, 3)),
             dma((chunks, 3)),
@@ -259,8 +267,8 @@
             dma((chunks, PAIR)),
             dma((chunks, PAIR)),
             dma((chunks, PAIR)),
-            dma((3,)),
-            dma((3,)),
+            dma((chunks, 3)),
+            dma((chunks, 3)),
         ],
         compiler_params=pltpu.CompilerParams(
             collective_id=0, has_side_effects=True, vmem_limit_bytes=60 * 1024 * 1024
@@ -269,6 +277,12 @@
         prompt.reshape(rows, width), forget_weight, value_weight, leak.reshape(1, here),
         query, next_input, read_gain.reshape(1, here),
     )
+    return pl.pallas_call(
+        hand_over,
+        out_shape=tuple(jax.ShapeDtypeStruct(a.shape, a.dtype) for a in made),
+        in_specs=[vm, vm],
+        out_specs=(vm, vm),
+    )(*made)
 
 
 def prefix(part, axis, combine, identity):

time: 37.3 us -> 34.8 us (0.933)
  local copies, waits for them, and re-layouts: 2.97 us -> 0 us
  Pallas kernels: 33.4 us -> 33.9 us
    unnamed x2 -> x0, local copies, waits for them, and re-layouts: 2.97 us -> none
    pallas_call x0 -> x1, Pallas kernels: none -> 1.68 us  [fused(): pl.pallas_call(hand_over, out_shape=tuple((jax.ShapeDtypeStruct(a.shape,...]
    pallas_call x1, Pallas kernels: 33.4 us -> 32.2 us  [fused(): pl.pallas_call(functools.partial(kernel, seqs, span, chunks), out_shape=(...]
where the time goes in v3:
time: 34.8 us; the launch traced here: 34.6 us
  Pallas kernels  33.9 us (97%)
  between operations  0.64 us (2%)
    pallas_call x1, Pallas kernels, fused(): pl.pallas_call(functools.partial(kernel, seqs, span, chunks), out_shape=(...  32.2 us
    pallas_call x1, Pallas kernels, fused(): pl.pallas_call(hand_over, out_shape=tuple((jax.ShapeDtypeStruct(a.shape,...  1.68 us

profile of v3, /device:TPU:0, one launch (start us, length us, event | category | flops | bytes accessed | tf_op | source)
XLA Modules:
  0.0 34.6 jit_solution(14571249372751147432)
XLA Ops:
  0.6 32.2 %shard_map.86 = (bf16[4,8,32,128]{3,2,1,0:T(8,128)(2,1)}, bf16[4,1024]{1,0:T(4,128)(2,1)}) custom-call(bf16[512,4096]{1,0:T(8,128)(2,1)} %bitcast.3, bf16[4096,1024]{1,0:T(8,128)(2,1)} %forget_w.1, bf16[4096,1024]{1,0:T(8,128)(2,1)} %value_w.1, f32[1,1024]{1,0:T(1,128)} %bitcast.4, bf16[4,1024]{1,0:T(4,128)(2,1)} %query.1, bf16[4,4096]{1,0:T(4,128)(2,1)} %nxt.1, ...), custom_call_target="tpu_custom_call" | custom-call | tf_op jit(solution)/shard_map/pallas_call | solution.py:239
  32.9 1.7 %shard_map.87 = (bf16[4,8,32,128]{3,2,1,0:T(8,128)(2,1)}, bf16[4,1024]{1,0:T(4,128)(2,1)}) custom-call(bf16[4,8,32,128]{3,2,1,0:T(8,128)(2,1)} %get-tuple-element.4.cache_in, bf16[4,1024]{1,0:T(4,128)(2,1)} %get-tuple-element.5.read_in), custom_call_target="tpu_custom_call" | custom-call | tf_op jit(solution)/shard_map/pallas_call | solution.py:280

commit v4 on v3

--- a/solution.py
+++ b/solution.py
@@ -11,7 +11,7 @@
 DV = 128
 PAIR = 2
 PAD = 16
-LAG = 3
+LAG = 4
 F32 = jnp.float32
 BF16 = jnp.bfloat16
 
@@ -131,18 +131,15 @@
         for source in range(1, count):
             part = totals[c, source]
             later = later * jnp.where(source > me, part, jnp.ones_like(part))
-        for s in range(seqs):
-            at = slice(s * span, (s + 1) * span)
-            to_end = jnp.concatenate(
-                [later[j * seqs + s : j * seqs + s + 1] for j in range(PAIR)], axis=1
-            )
-            weighted = (keys_v[c % 2, at, :] * to_end).astype(BF16)
-            weighed = weighted.astype(F32) * qf_v[s : s + 1, cols(c)]
-            for j in range(PAIR):
-                head = slice(j * DK, (j + 1) * DK)
-                v = val_v[at, head]
+        for j in range(PAIR):
+            head = slice(j * DK, (j + 1) * DK)
+            for s in range(seqs):
+                at = slice(s * span, (s + 1) * span)
+                row = j * seqs + s
+                weighted = (keys_v[c % 2, at, head] * later[row : row + 1]).astype(BF16)
+                keys_v[c % 2, at, head] = weighted.astype(F32)
                 state = lax.dot_general(
-                    weighted[:, head], v, (((0,), (0,)), ((), ())),
+                    weighted, val_v[at, head], (((0,), (0,)), ((), ())),
                     preferred_element_type=F32,
                 )
                 for owner in range(count):
@@ -150,12 +147,16 @@
                     states[c, j, first, second, s * kdev : (s + 1) * kdev, :] = state[
                         owner * kdev : (owner + 1) * kdev
                     ]
+            s1_copy(c, j).start()
+        for s in range(seqs):
+            at = slice(s * span, (s + 1) * span)
+            weighed = keys_v[c % 2, at, :] * qf_v[s : s + 1, cols(c)]
+            for j in range(PAIR):
+                head = slice(j * DK, (j + 1) * DK)
                 a = jnp.sum(weighed[:, head], axis=1, keepdims=True)
                 reads[c, me, j * seqs + s : j * seqs + s + 1, :] = jnp.sum(
-                    a * v.astype(F32), axis=0, keepdims=True
+                    a * val_v[at, head].astype(F32), axis=0, keepdims=True
                 )
-        for j in range(PAIR):
-            s1_copy(c, j).start()
         for i in range(3):
             read_copy(c, i).start()
 

time: 34.8 us -> 35.6 us (1.023)
  Pallas kernels: 33.9 us -> 34.7 us
    pallas_call x1, Pallas kernels: 32.2 us -> 33.1 us  [fused(): pl.pallas_call(functools.partial(kernel, seqs, span, chunks), out_shape=(...]
where the time goes in v4:
time: 35.6 us; the launch traced here: 35.4 us
  Pallas kernels  34.7 us (97%)
  between operations  0.64 us (2%)
    pallas_call x1, Pallas kernels, fused(): pl.pallas_call(functools.partial(kernel, seqs, span, chunks), out_shape=(...  33.1 us
    pallas_call x1, Pallas kernels, fused(): pl.pallas_call(hand_over, out_shape=tuple((jax.ShapeDtypeStruct(a.shape,...  1.68 us

profile of v4, /device:TPU:0, one launch (start us, length us, event | category | flops | bytes accessed | tf_op | source)
XLA Modules:
  0.0 35.4 jit_solution(5477005952661312104)
XLA Ops:
  0.6 33.1 %shard_map.86 = (bf16[4,8,32,128]{3,2,1,0:T(8,128)(2,1)}, bf16[4,1024]{1,0:T(4,128)(2,1)}) custom-call(bf16[512,4096]{1,0:T(8,128)(2,1)} %bitcast.3, bf16[4096,1024]{1,0:T(8,128)(2,1)} %forget_w.1, bf16[4096,1024]{1,0:T(8,128)(2,1)} %value_w.1, f32[1,1024]{1,0:T(1,128)} %bitcast.4, bf16[4,1024]{1,0:T(4,128)(2,1)} %query.1, bf16[4,4096]{1,0:T(4,128)(2,1)} %nxt.1, ...), custom_call_target="tpu_custom_call" | custom-call | tf_op jit(solution)/shard_map/pallas_call | solution.py:240
  33.7 1.7 %shard_map.87 = (bf16[4,8,32,128]{3,2,1,0:T(8,128)(2,1)}, bf16[4,1024]{1,0:T(4,128)(2,1)}) custom-call(bf16[4,8,32,128]{3,2,1,0:T(8,128)(2,1)} %get-tuple-element.4.cache_in, bf16[4,1024]{1,0:T(4,128)(2,1)} %get-tuple-element.5.read_in), custom_call_target="tpu_custom_call" | custom-call | tf_op jit(solution)/shard_map/pallas_call | solution.py:281

commit v5 on v3

--- a/solution.py
+++ b/solution.py
@@ -11,7 +11,7 @@
 DV = 128
 PAIR = 2
 PAD = 16
-LAG = 3
+LAG = 4
 F32 = jnp.float32
 BF16 = jnp.bfloat16
 

time: 34.8 us -> 34.6 us (level)
  no operation moved by 1% of the time
where the time goes in v5:
time: 34.6 us; the launch traced here: 34.4 us
  Pallas kernels  33.7 us (97%)
  between operations  0.64 us (2%)
    pallas_call x1, Pallas kernels, fused(): pl.pallas_call(functools.partial(kernel, seqs, span, chunks), out_shape=(...  32.1 us
    pallas_call x1, Pallas kernels, fused(): pl.pallas_call(hand_over, out_shape=tuple((jax.ShapeDtypeStruct(a.shape,...  1.68 us

profile of v5, /device:TPU:0, one launch (start us, length us, event | category | flops | bytes accessed | tf_op | source)
XLA Modules:
  0.0 34.4 jit_solution(5456130831957365744)
XLA Ops:
  0.6 32.1 %shard_map.86 = (bf16[4,8,32,128]{3,2,1,0:T(8,128)(2,1)}, bf16[4,1024]{1,0:T(4,128)(2,1)}) custom-call(bf16[512,4096]{1,0:T(8,128)(2,1)} %bitcast.3, bf16[4096,1024]{1,0:T(8,128)(2,1)} %forget_w.1, bf16[4096,1024]{1,0:T(8,128)(2,1)} %value_w.1, f32[1,1024]{1,0:T(1,128)} %bitcast.4, bf16[4,1024]{1,0:T(4,128)(2,1)} %query.1, bf16[4,4096]{1,0:T(4,128)(2,1)} %nxt.1, ...), custom_call_target="tpu_custom_call" | custom-call | tf_op jit(solution)/shard_map/pallas_call | solution.py:239
  32.7 1.7 %shard_map.87 = (bf16[4,8,32,128]{3,2,1,0:T(8,128)(2,1)}, bf16[4,1024]{1,0:T(4,128)(2,1)}) custom-call(bf16[4,8,32,128]{3,2,1,0:T(8,128)(2,1)} %get-tuple-element.4.cache_in, bf16[4,1024]{1,0:T(4,128)(2,1)} %get-tuple-element.5.read_in), custom_call_target="tpu_custom_call" | custom-call | tf_op jit(solution)/shard_map/pallas_call | solution.py:280
